TPU v7x, 32 devices: a whole 2x2x4 slice. The times are simulated.
32 devices in a mesh: sp: 16 (over z, y, core), tp: 2 (over x).
Axes of the slice: x: 2, y: 2, z: 4, core: 2. Of those that a mesh axis runs over, the one named last changes fastest.
Arguments:
- inputs: bfloat16 [4096, 4096], P('sp', 'tp'), may hold values from -20 to 20
- norm_gain: float32 [3, 4096], replicated, may hold values from 0.1 to 1.9
- in_weight: bfloat16 [3, 4096, 1024], P(None, 'tp', 'sp'), may hold values from -0.09375 to 0.09375
- pool_scale: float32 [3, 1024], replicated, may hold values from 0.1 to 1.9
- out_weight: bfloat16 [3, 1024, 4096], P(None, 'sp', 'tp'), may hold values from -0.1875 to 0.1875
Outputs:
- final_state: bfloat16 [4096, 4096], P('sp', 'tp')
All inputs are finite; a program needn't handle non-finite values.
Results may differ from a plain program's by a relative error of at most 0.017.
Values may be sent and summed in bfloat16 or wider, within the bound.
A program may use at most 64 MiB of HBM per device.

v0:
```python
import jax
import jax.numpy as jnp
from jax import lax
from jax.sharding import PartitionSpec as P

D = 4096
P_SIZE = 1024
LAYERS = 3


epsilon = 1e-06
halo_rows = 16
group_count = 4


def from_behind(value, axis, steps):
    count = lax.axis_size(axis)
    initial, last = (max(0, -steps), min(count, count - steps))
    return lax.ppermute(value, axis, [(source, source + steps) for source in range(initial, last)])


def window_means(extended, row_count, first_channel, first_pos, pool_total):
    width = extended.shape[1]
    channel = first_channel + lax.broadcasted_iota(jnp.int32, (1, width), 1)
    group_index = channel // (pool_total // group_count)
    window_len = jnp.left_shift(jnp.int32(2), group_index)
    running = jnp.zeros((row_count, width), jnp.float32)
    for offset in range(halo_rows):
        shifted = extended[halo_rows - offset : halo_rows - offset + row_count]
        running = running + jnp.where(offset < window_len, shifted, 0.0)
    position = first_pos + lax.broadcasted_iota(jnp.int32, (row_count, 1), 0)
    divisor = jnp.minimum(position + 1, window_len).astype(jnp.float32)
    return running / divisor - extended[halo_rows:]


def body(inputs, norm_gain, in_weight, pool_scale, out_weight):
    row_count, feature_part = inputs.shape
    channel_part = P_SIZE // lax.axis_size("tp")
    tp_index = lax.axis_index("tp")
    sp_index = lax.axis_index("sp")
    current = inputs
    in_all, out_all = (
        lax.all_gather(in_weight, "sp", axis=2, tiled=True),
        lax.all_gather(out_weight, "sp", axis=1, tiled=True),
    )
    for layer_index in range(LAYERS):
        gain_row = norm_gain[layer_index]
        widened = current.astype(jnp.float32)
        squares = lax.psum(jnp.sum(widened * widened, axis=1), "tp")
        inv_rms = lax.rsqrt(squares / D + epsilon)[:, None]
        own_gain = lax.dynamic_slice_in_dim(gain_row, tp_index * feature_part, feature_part)
        normed = (widened * inv_rms * own_gain).astype(jnp.bfloat16)
        partials = jnp.dot(normed, in_all[layer_index], preferred_element_type=jnp.float32)
        pool_in = lax.psum_scatter(
            partials.astype(jnp.bfloat16), "tp", scatter_dimension=1, tiled=True
        )
        edge_block = from_behind(pool_in[row_count - halo_rows :], "sp", 1)
        extended = jnp.concatenate([edge_block, pool_in], 0).astype(jnp.float32)
        means = window_means(
            extended, row_count, tp_index * channel_part, sp_index * row_count, P_SIZE
        )
        own_scale = lax.dynamic_slice_in_dim(
            pool_scale[layer_index], tp_index * channel_part, channel_part
        )
        mixed = (means * own_scale).astype(jnp.bfloat16)
        all_pooled = lax.all_gather(mixed, "tp", axis=1, tiled=True)
        branch = jnp.dot(all_pooled, out_all[layer_index], preferred_element_type=jnp.float32)
        current = (current.astype(jnp.float32) + branch).astype(jnp.bfloat16)
    return current


def solution(mesh):
    placed = (P("sp", "tp"), P(), P(None, "tp", "sp"), P(), P(None, "sp", "tp"))
    return jax.shard_map(body, mesh=mesh, in_specs=placed, out_specs=P("sp", "tp"), check_vma=False)
```

profile of v0, /device:TPU:4, one launch (start us, length us, event | category | flops | bytes accessed | tf_op | source)
XLA Modules:
  0.0 327.6 jit_solution(14062841679788952662)
XLA Ops:
  6.5 0.0 all-gather.3.cloned.1.call-start
  6.5 0.7 all-gather.3.cloned.1.call-update
  7.3 0.0 reduce-scatter.4.cloned.1.call-start
  7.3 1.5 fusion.9
  8.8 4.9 %psum.21 = f32[256]{0:T(256)S(1)} all-reduce(f32[256]{0:T(256)S(1)} %fusion.9), channel_id=1, replica_groups=mesh['sp'=16,'tp'=2] {'tp'}, use_global_device_ids=true, to_apply=%region_1.0 | all-reduce | flops 256 | bytes 2048 | tf_op jit(solution)/shard_map/psum | solution.py:49
  13.8 1.0 fusion.91
  14.8 95.5 %all-gather.3.cloned.1.call-done = bf16[3,2048,1024]{1,2,0:T(8,128)(2,1)} async-done(((bf16[3,2048,64]{1,2,0:T(8,128)(2,1)}), bf16[3,2048,1024]{1,2,0:T(8,128)(2,1)}) %all-gather.3.cloned.1.call-update) | async-done | bytes 12582928 | tf_op jit(solution)/shard_map/all_gather | solution.py:43
  110.3 0.0 copy-start.1
  110.3 4.6 %fusion.18 = bf16[256,1024]{1,0:T(8,128)(2,1)} fusion(bf16[3,2048,1024]{1,2,0:T(8,128)(2,1)} %all-gather.3.cloned.1.call-done, bf16[256,2048]{1,0:T(8,128)(2,1)} %param.5, f32[2048]{0:T(1024)S(1)} %bitcast.54, f32[256]{0:T(256)S(1)} %add_rsqrt_fusion.2), kind=kOutput, calls=%fused_computation.33 | convolution fusion | flops 1076101120 | bytes 5776384 | tf_op jit(solution)/shard_map/dot_general | solution.py:53
  114.9 0.0 reduce-scatter.4.cloned.1.call-update
  114.9 0.0 all-gather.5.cloned.1.call-start
  115.0 0.7 all-gather.5.cloned.1.call-update
  115.7 0.0 reduce-scatter.6.cloned.1.call-start
  115.9 0.0 copy-done.1
  116.0 12.9 %reduce-scatter.4.cloned.1.call-done = bf16[256,512]{1,0:T(8,128)(2,1)} async-done(((bf16[256,1024]{1,0:T(8,128)(2,1)}), bf16[256,512]{1,0:T(8,128)(2,1)}) %reduce-scatter.4.cloned.1.call-update) | async-done | bytes 262160 | tf_op jit(solution)/shard_map/reduce_scatter | solution.py:54
  128.9 0.7 slice.256
  129.6 1.9 collective-permute-start
  131.5 3.1 collective-permute-done
  134.6 1.0 maximum_convert_fusion
  135.6 0.0 copy-start
  135.7 1.2 fusion.84
  136.8 8.2 %all_gather.16 = bf16[256,1024]{1,0:T(8,128)(2,1)S(1)} all-gather(bf16[256,512]{1,0:T(8,128)(2,1)S(1)} %fusion.84), channel_id=1, replica_groups=mesh['sp'=16,'tp'=2] {'tp'}, dimensions={1}, use_global_device_ids=true | all-gather | bytes 786432 | tf_op jit(solution)/shard_map/all_gather | solution.py:66
  145.0 85.6 %all-gather.5.cloned.1.call-done = bf16[3,1024,2048]{2,1,0:T(8,128)(2,1)} async-done(((bf16[3,64,2048]{2,1,0:T(8,128)(2,1)}), bf16[3,1024,2048]{2,1,0:T(8,128)(2,1)}) %all-gather.5.cloned.1.call-update) | async-done | bytes 12582928 | tf_op jit(solution)/shard_map/all_gather | solution.py:44
  230.6 0.0 copy-done
  230.6 3.6 %fusion.12 = (f32[256]{0:T(256)S(1)}, bf16[256,2048]{1,0:T(8,128)(2,1)S(1)}) fusion(bf16[256,1024]{1,0:T(8,128)(2,1)S(1)} %all_gather.16, bf16[3,1024,2048]{2,1,0:T(8,128)(2,1)} %all-gather.5.cloned.1.call-done, bf16[256,2048]{1,0:T(8,128)(2,1)S(1)} %copy-done), kind=kOutput, calls=%fused_computation.27 | convolution fusion | flops 1076887296 | bytes 6816768 | tf_op jit(solution)/shard_map/dot_general | solution.py:67
  234.3 4.9 %psum.22 = f32[256]{0:T(256)S(1)} all-reduce(f32[256]{0:T(256)S(1)} %get-tuple-element.11), channel_id=1, replica_groups=mesh['sp'=16,'tp'=2] {'tp'}, use_global_device_ids=true, to_apply=%region_4.5 | all-reduce | flops 256 | bytes 2048 | tf_op jit(solution)/shard_map/psum | solution.py:49
  239.2 4.3 %fusion.19 = bf16[256,1024]{1,0:T(8,128)(2,1)} fusion(bf16[3,2048,1024]{1,2,0:T(8,128)(2,1)} %all-gather.3.cloned.1.call-done, bf16[256,2048]{1,0:T(8,128)(2,1)S(1)} %get-tuple-element.12, f32[2048]{0:T(1024)S(1)} %bitcast.52, f32[256]{0:T(256)S(1)} %add_rsqrt_fusion.1), kind=kOutput, calls=%fused_computation.34 | convolution fusion | flops 1076101120 | bytes 5776384 | tf_op jit(solution)/shard_map/dot_general | solution.py:53
  243.5 0.0 reduce-scatter.6.cloned.1.call-update
  243.5 0.0 reduce-scatter.8.cloned.1.call-start
  243.6 13.9 %reduce-scatter.6.cloned.1.call-done = bf16[256,512]{1,0:T(8,128)(2,1)} async-done(((bf16[256,1024]{1,0:T(8,128)(2,1)}), bf16[256,512]{1,0:T(8,128)(2,1)}) %reduce-scatter.6.cloned.1.call-update) | async-done | bytes 262160 | tf_op jit(solution)/shard_map/reduce_scatter | solution.py:54
  257.5 0.7 slice.275
  258.2 1.9 collective-permute-start.1
  260.1 3.1 collective-permute-done.1
  263.2 1.0 maximum_convert_fusion.1
  264.2 1.2 fusion.85
  265.4 8.2 %all_gather.18 = bf16[256,1024]{1,0:T(8,128)(2,1)S(1)} all-gather(bf16[256,512]{1,0:T(8,128)(2,1)S(1)} %fusion.85), channel_id=1, replica_groups=mesh['sp'=16,'tp'=2] {'tp'}, dimensions={1}, use_global_device_ids=true | all-gather | bytes 786432 | tf_op jit(solution)/shard_map/all_gather | solution.py:66
  273.6 3.7 %fusion.15 = (f32[256]{0:T(256)S(1)}, bf16[256,2048]{1,0:T(8,128)(2,1)S(1)}) fusion(bf16[256,1024]{1,0:T(8,128)(2,1)S(1)} %all_gather.18, bf16[3,1024,2048]{2,1,0:T(8,128)(2,1)} %all-gather.5.cloned.1.call-done, bf16[256,2048]{1,0:T(8,128)(2,1)S(1)} %get-tuple-element.12), kind=kOutput, calls=%fused_computation.30 | convolution fusion | flops 1076887296 | bytes 6816768 | tf_op jit(solution)/shard_map/dot_general | solution.py:67
  277.2 4.9 %psum.23 = f32[256]{0:T(256)S(1)} all-reduce(f32[256]{0:T(256)S(1)} %get-tuple-element.13), channel_id=1, replica_groups=mesh['sp'=16,'tp'=2] {'tp'}, use_global_device_ids=true, to_apply=%region_7.8 | all-reduce | flops 256 | bytes 2048 | tf_op jit(solution)/shard_map/psum | solution.py:49
  282.2 4.4 %fusion.20 = bf16[256,1024]{1,0:T(8,128)(2,1)} fusion(bf16[3,2048,1024]{1,2,0:T(8,128)(2,1)} %all-gather.3.cloned.1.call-done, bf16[256,2048]{1,0:T(8,128)(2,1)S(1)} %get-tuple-element.14, f32[2048]{0:T(1024)S(1)} %bitcast.53, f32[256]{0:T(256)S(1)} %add_rsqrt_fusion), kind=kOutput, calls=%fused_computation.35 | convolution fusion | flops 1076101120 | bytes 5776384 | tf_op jit(solution)/shard_map/dot_general | solution.py:53
  286.6 0.0 reduce-scatter.8.cloned.1.call-update
  286.6 13.9 %reduce-scatter.8.cloned.1.call-done = bf16[256,512]{1,0:T(8,128)(2,1)} async-done(((bf16[256,1024]{1,0:T(8,128)(2,1)}), bf16[256,512]{1,0:T(8,128)(2,1)}) %reduce-scatter.8.cloned.1.call-update) | async-done | bytes 262160 | tf_op jit(solution)/shard_map/reduce_scatter | solution.py:54
  300.5 0.7 slice.294
  301.2 1.9 collective-permute-start.2
  303.1 3.1 collective-permute-done.2
  306.3 1.0 maximum_convert_fusion.2
  307.3 1.2 fusion.86
  308.5 8.2 %all_gather.19 = bf16[256,1024]{1,0:T(8,128)(2,1)S(1)} all-gather(bf16[256,512]{1,0:T(8,128)(2,1)S(1)} %fusion.86), channel_id=1, replica_groups=mesh['sp'=16,'tp'=2] {'tp'}, dimensions={1}, use_global_device_ids=true | all-gather | bytes 786432 | tf_op jit(solution)/shard_map/all_gather | solution.py:66
  316.6 4.4 %fusion.8 = bf16[256,2048]{1,0:T(8,128)(2,1)} fusion(bf16[256,1024]{1,0:T(8,128)(2,1)S(1)} %all_gather.19, bf16[3,1024,2048]{2,1,0:T(8,128)(2,1)} %all-gather.5.cloned.1.call-done, bf16[256,2048]{1,0:T(8,128)(2,1)S(1)} %get-tuple-element.14), kind=kOutput, calls=%fused_computation.23 | convolution fusion | flops 1075314688 | bytes 6815744 | tf_op jit(solution)/shard_map/dot_general | solution.py:67
  (20 shorter events, 0.2 us)
Async XLA Ops:
  6.5 103.8 %all-gather.3.cloned.1.call-start = ((), (), s32[]{:S(2)}) async-start(), calls=%async_computation.3 | async-start | bytes 13369344 | tf_op jit(solution)/shard_map/all_gather | solution.py:43
  7.3 121.6 %reduce-scatter.4.cloned.1.call-start = ((), (), s32[]{:S(2)}) async-start(), calls=%async_computation.4 | async-start | bytes 786432 | tf_op jit(solution)/shard_map/reduce_scatter | solution.py:54
  110.3 5.6 %copy-start.1 = (f32[3,1024]{1,0:T(4,128)S(1)}, f32[3,1024]{1,0:T(4,128)}, u32[]{:S(2)}) copy-start(f32[3,1024]{1,0:T(4,128)} %param.8) | copy-start | bytes 36868
  114.9 115.7 %all-gather.5.cloned.1.call-start = ((), (), s32[]{:S(2)}) async-start(), calls=%async_computation.5 | async-start | bytes 13369344 | tf_op jit(solution)/shard_map/all_gather | solution.py:44
  115.7 141.8 %reduce-scatter.6.cloned.1.call-start = ((), (), s32[]{:S(2)}) async-start(), calls=%async_computation.6 | async-start | bytes 786432 | tf_op jit(solution)/shard_map/reduce_scatter | solution.py:54
  129.6 5.0 %collective-permute-start = (bf16[16,512]{1,0:T(8,128)(2,1)S(1)}, bf16[16,512]{1,0:T(8,128)(2,1)S(1)}, u32[]{:S(2)}, u32[]{:S(2)}) collective-permute-start(bf16[16,512]{1,0:T(8,128)(2,1)S(1)} %slice.256), channel_id=1, source_target_pairs={{0,2},{2,4},{4,6},{6,8},{8,10},{10,12},{12,14},{14,16},{16,18},{18... | collective-permute-start | bytes 49160 | tf_op jit(solution)/shard_map/ppermute | solution.py:19
  135.6 95.0 %copy-start = (bf16[256,2048]{1,0:T(8,128)(2,1)S(1)}, bf16[256,2048]{1,0:T(8,128)(2,1)}, u32[]{:S(2)}) copy-start(bf16[256,2048]{1,0:T(8,128)(2,1)} %param.5) | copy-start | bytes 3145732
  243.5 57.0 %reduce-scatter.8.cloned.1.call-start = ((), (), s32[]{:S(2)}) async-start(), calls=%async_computation.7 | async-start | bytes 786432 | tf_op jit(solution)/shard_map/reduce_scatter | solution.py:54
  258.2 5.0 %collective-permute-start.1 = (bf16[16,512]{1,0:T(8,128)(2,1)S(1)}, bf16[16,512]{1,0:T(8,128)(2,1)S(1)}, u32[]{:S(2)}, u32[]{:S(2)}) collective-permute-start(bf16[16,512]{1,0:T(8,128)(2,1)S(1)} %slice.275), channel_id=1, source_target_pairs={{0,2},{2,4},{4,6},{6,8},{8,10},{10,12},{12,14},{14,16},{16,18},{18... | collective-permute-start | bytes 49160 | tf_op jit(solution)/shard_map/ppermute | solution.py:19
  301.2 5.0 %collective-permute-start.2 = (bf16[16,512]{1,0:T(8,128)(2,1)S(1)}, bf16[16,512]{1,0:T(8,128)(2,1)S(1)}, u32[]{:S(2)}, u32[]{:S(2)}) collective-permute-start(bf16[16,512]{1,0:T(8,128)(2,1)S(1)} %slice.294), channel_id=1, source_target_pairs={{0,2},{2,4},{4,6},{6,8},{8,10},{10,12},{12,14},{14,16},{16,18},{18... | collective-permute-start | bytes 49160 | tf_op jit(solution)/shard_map/ppermute | solution.py:19
Sparse Core Ops, SparseCore 0:
  9.5 100.7 all-gather.2
  115.1 13.7 reduce-scatter.3
  131.1 99.5 all-gather.4
  243.7 13.7 reduce-scatter.5
  286.7 13.7 reduce-scatter.7
where the time goes:
time: 328 us
  waiting for transfers between devices  233 us (71%)
  blocking collectives  39.3 us (12%)
  matrix products  25 us (8%)
  between operations  13.3 us (4%)
  other arithmetic  8.23 us (3%)
  starting transfers between devices  5.89 us (2%)
    all_gather x1, waiting for transfers between devices, body(): lax.all_gather(in_weight, 'sp', axis=2, tiled=True)  95.5 us
    all_gather x1, waiting for transfers between devices, body(): lax.all_gather(out_weight, 'sp', axis=1, tiled=True)  85.6 us
    reduce_scatter x3, waiting for transfers between devices, body(): lax.psum_scatter(partials.astype(jnp.bfloat16), 'tp', scatter_dimension=1...  40.7 us
    all_gather x3, blocking collectives, body(): all_pooled = lax.all_gather(mixed, 'tp', axis=1, tiled=True)  24.5 us
    psum x3, blocking collectives, body(): squares = lax.psum(jnp.sum(widened * widened, axis=1), 'tp')  14.8 us
    dot_general x3, matrix products, body(): jnp.dot(normed, in_all[layer_index], preferred_element_type=jnp.float32)  13.3 us
    dot_general x3, matrix products, body(): jnp.dot(all_pooled, out_all[layer_index], preferred_element_type=jnp.floa...  11.7 us
    ppermute x3, waiting for transfers between devices, from_behind(): lax.ppermute(value, axis, [(source, source + steps) for source in range(i...  9.34 us
  transfers between devices with their start and end apart: 8, of which 8 were waited for; matrix products, arithmetic and copies ran while one was open for 2% of the time, Pallas kernels for 0%

commit v1 on v0

v1 whole, which is shorter than its diff:
```python
import functools

import jax
import jax.numpy as jnp
from jax import lax
from jax.experimental import pallas as pl
from jax.experimental.pallas import tpu as pltpu
from jax.sharding import PartitionSpec as P

EPS = 1e-06
REACH = 16
GROUPS = 4
MESH_ID = pl.DeviceIdType.MESH


def shift_sp(value):
    count = lax.axis_size("sp")
    return lax.ppermute(value, "sp", [(i, i + 1) for i in range(count - 1)])


def window_means(extended, row_count, first_channel, first_pos, pool_total):
    width = extended.shape[1]
    channel = first_channel + lax.broadcasted_iota(jnp.int32, (1, width), 1)
    window_len = jnp.left_shift(jnp.int32(2), channel // (pool_total // GROUPS))
    running = jnp.zeros((row_count, width), jnp.float32)
    for offset in range(REACH):
        shifted = extended[REACH - offset : REACH - offset + row_count]
        running = running + jnp.where(offset < window_len, shifted, 0.0)
    position = first_pos + lax.broadcasted_iota(jnp.int32, (row_count, 1), 0)
    divisor = jnp.minimum(position + 1, window_len).astype(jnp.float32)
    return running / divisor - extended[REACH:]


def plain_body(inputs, norm_gain, in_weight, pool_scale, out_weight):
    rows, feats = inputs.shape
    layers, features = norm_gain.shape
    pools = pool_scale.shape[1]
    part = pools // lax.axis_size("tp")
    t = lax.axis_index("tp")
    s = lax.axis_index("sp")
    current = inputs
    for layer in range(layers):
        in_all = lax.all_gather(in_weight[layer], "sp", axis=1, tiled=True)
        out_all = lax.all_gather(out_weight[layer], "sp", axis=0, tiled=True)
        wide = current.astype(jnp.float32)
        squares = lax.psum(jnp.sum(wide * wide, axis=1), "tp")
        inv_rms = lax.rsqrt(squares / features + EPS)[:, None]
        gain = lax.dynamic_slice_in_dim(norm_gain[layer], t * feats, feats)
        normed = (wide * inv_rms * gain).astype(jnp.bfloat16)
        partial = jnp.dot(normed, in_all, preferred_element_type=jnp.float32)
        pool_in = lax.psum_scatter(
            partial.astype(jnp.bfloat16), "tp", scatter_dimension=1, tiled=True
        )
        edge = shift_sp(pool_in[rows - REACH :])
        extended = jnp.concatenate([edge, pool_in], 0).astype(jnp.float32)
        means = window_means(extended, rows, t * part, s * rows, pools)
        scale = lax.dynamic_slice_in_dim(pool_scale[layer], t * part, part)
        mixed = (means * scale).astype(jnp.bfloat16)
        pooled = lax.all_gather(mixed, "tp", axis=1, tiled=True)
        branch = jnp.dot(pooled, out_all, preferred_element_type=jnp.float32)
        current = (current.astype(jnp.float32) + branch).astype(jnp.bfloat16)
    return current


def kernel(
    n_z, layers, halo,
    x_ref, gain_ref, wi_ref, scale_ref, wo_ref, o_ref,
    held, state, xg, edge, p_own, p_send, p_recv, mix, sq_send, sq_recv,
    w_send, w_recv, local_sem, a_send, a_recv,
):
    rows, feats = x_ref.shape
    total = rows + halo
    blocks = held.shape[1]
    half = mix.shape[3]
    pools = 2 * half
    phases = 2 * layers
    s = lax.axis_index("sp")
    t = lax.axis_index("tp")
    core = s % 2
    y = (s // 2) % 2
    z = s // 4

    def block_of(zz, yy, cc):
        return zz * 4 + yy * 2 + cc

    zs = [(z + d) % n_z for d in range(n_z)]
    y_mate = (block_of(z, 1 - y, core), t)
    c_mate = (block_of(z, y, 1 - core), t)
    x_mate = (s, 1 - t)
    after = ((s + 1) % blocks, t)
    before = ((s + blocks - 1) % blocks, t)
    z_mates = [(block_of(zz, y, core), t) for zz in zs[1:]]

    barrier = pltpu.get_barrier_semaphore()
    peers = z_mates + [y_mate, c_mate, x_mate, after, before]
    for peer in peers:
        pl.semaphore_signal(barrier, inc=1, device_id=peer, device_id_type=MESH_ID)
    pl.semaphore_wait(barrier, len(peers))

    sent = []

    def send(src, dst, send_sem, recv_sem, to):
        copy = pltpu.make_async_remote_copy(
            src_ref=src, dst_ref=dst, send_sem=send_sem, recv_sem=recv_sem,
            device_id=to, device_id_type=MESH_ID,
        )
        copy.start()
        sent.append(copy)

    def arrived(ref, sem):
        pltpu.make_async_remote_copy(
            src_ref=ref, dst_ref=ref, send_sem=sem, recv_sem=sem,
            device_id=c_mate, device_id_type=MESH_ID,
        ).wait_recv()

    def own(p):
        return (wi_ref if p % 2 == 0 else wo_ref).at[p // 2]

    count = [0] * phases

    def send_block(p, src, block, to):
        send(src, held.at[p, block], w_send.at[p, count[p]], w_recv.at[p, block], to)
        count[p] += 1

    def wait_block(p, block):
        arrived(held.at[p, block], w_recv.at[p, block])

    locals_ = []

    def issue_own(p):
        if p >= phases:
            return
        for mate in z_mates:
            send_block(p, own(p), s, mate)
        send_block(p, own(p), s, y_mate)
        send_block(p, own(p), s, c_mate)
        copy = pltpu.make_async_copy(own(p), held.at[p, s], local_sem.at[p])
        copy.start()
        locals_.append(copy)

    def pump_z(p):
        if p >= phases:
            return
        for zz in [zs[1], zs[-1]] + zs[2:-1]:
            block = block_of(zz, y, core)
            wait_block(p, block)
            send_block(p, held.at[p, block], block, y_mate)
            send_block(p, held.at[p, block], block, c_mate)

    def pump_y(p):
        for zz in [zs[0], zs[1], zs[-1]] + zs[2:-1]:
            block = block_of(zz, 1 - y, core)
            wait_block(p, block)
            send_block(p, held.at[p, block], block, c_mate)

    def finish(p):
        locals_[p].wait()
        for zz in zs:
            for yy in (y, 1 - y):
                wait_block(p, block_of(zz, yy, 1 - core))

    send(x_ref.at[pl.ds(rows - halo, halo)], edge, a_send.at[0], a_recv.at[0], after)
    issue_own(0)
    issue_own(1)

    @pl.loop(0, rows // REACH)
    def _(i):
        state[pl.ds(halo + i * REACH, REACH)] = x_ref[pl.ds(i * REACH, REACH)]

    arrived(edge, a_recv.at[0])
    keep = (s > 0).astype(jnp.float32)

    @pl.loop(0, halo // REACH)
    def _(i):
        part = edge[pl.ds(i * REACH, REACH)].astype(jnp.float32) * keep
        state[pl.ds(i * REACH, REACH)] = part.astype(jnp.bfloat16)

    def squares(layer):
        @pl.loop(0, total // REACH)
        def _(i):
            at = pl.ds(i * REACH, REACH)
            wide = state[at].astype(jnp.float32)
            value = jnp.sum(wide * wide, axis=1, keepdims=True)
            sq_send[layer, at] = jnp.broadcast_to(value, (REACH, 128))
            gain = gain_ref[pl.ds(layer, 1), pl.ds(pl.multiple_of(t * feats, 128), feats)]
            xg[at] = (wide * gain).astype(jnp.bfloat16)

        send(sq_send.at[layer], sq_recv.at[layer], a_send.at[1 + 3 * layer],
             a_recv.at[1 + 3 * layer], x_mate)

    def project(p, which):
        part = held[p, pl.ds(which * (blocks // 2), blocks // 2)].reshape(half, feats)
        return lax.dot_general(
            xg[...], part, (((1,), (1,)), ((), ())), preferred_element_type=jnp.float32
        )

    def compute_in(layer):
        p = 2 * layer
        sem = 2 + 3 * layer
        p_send[layer] = project(p, 1 - t).astype(jnp.bfloat16)
        send(p_send.at[layer], p_recv.at[layer], a_send.at[sem], a_recv.at[sem], x_mate)
        p_own[...] = project(p, t)
        arrived(sq_recv.at[layer], a_recv.at[sem - 1])
        arrived(p_recv.at[layer], a_recv.at[sem])
        lanes = 128
        row = lax.broadcasted_iota(jnp.int32, (total, lanes), 0)
        position = s * rows - halo + row
        mean = (sq_send[layer] + sq_recv[layer]) / (2 * feats)
        inv = lax.rsqrt(mean + EPS)
        for j in range(half // lanes):
            cols = pl.ds(j * lanes, lanes)
            joined = p_own[:, cols].astype(jnp.bfloat16).astype(jnp.float32)
            joined = joined + p_recv[layer, :, cols].astype(jnp.float32)
            base = (joined * inv).astype(jnp.bfloat16).astype(jnp.float32)
            channel = t * half + j * lanes + lax.broadcasted_iota(jnp.int32, (1, lanes), 1)
            group = channel // (pools // GROUPS)
            running = base
            width = 1
            picked = None
            for g in range(GROUPS):
                running = running + pltpu.roll(running, width, 0)
                width *= 2
                picked = running if picked is None else jnp.where(group >= g, running, picked)
            span = jnp.left_shift(jnp.int32(2), group)
            divisor = jnp.maximum(jnp.minimum(position + 1, span), 1).astype(jnp.float32)
            scale = scale_ref[
                pl.ds(layer, 1), pl.ds(pl.multiple_of(t * half + j * lanes, 128), lanes)
            ]
            mix[layer, t, :, cols] = ((picked / divisor - base) * scale).astype(jnp.bfloat16)
        send(mix.at[layer, t], mix.at[layer, t], a_send.at[sem + 1], a_recv.at[sem + 1], x_mate)

    def compute_out(layer):
        p = 2 * layer + 1
        sem = 3 + 3 * layer
        arrived(mix.at[layer, 1 - t], a_recv.at[sem])
        width = 256
        last = layer == layers - 1

        @pl.loop(0, feats // width)
        def _(n):
            cols = pl.ds(pl.multiple_of(n * width, width), width)
            low = held[p, pl.ds(0, blocks // 2), :, cols].reshape(half, width)
            high = held[p, pl.ds(blocks // 2, blocks // 2), :, cols].reshape(half, width)
            branch = jnp.dot(mix[layer, 0], low, preferred_element_type=jnp.float32)
            branch = branch + jnp.dot(mix[layer, 1], high, preferred_element_type=jnp.float32)
            new = (state[:, cols].astype(jnp.float32) + branch).astype(jnp.bfloat16)
            if last:
                o_ref[:, cols] = new[halo:]
            else:
                state[:, cols] = new

    squares(0)
    pump_z(0)
    for p in range(phases):
        issue_own(p + 2)
        pump_z(p + 1)
        pump_y(p)
        finish(p)
        if p % 2 == 0:
            compute_in(p // 2)
        else:
            compute_out(p // 2)
            if p // 2 + 1 < layers:
                squares(p // 2 + 1)
    for copy in sent:
        copy.wait_send()


def fused_body(inputs, norm_gain, in_weight, pool_scale, out_weight):
    rows, feats = inputs.shape
    layers = norm_gain.shape[0]
    half = pool_scale.shape[1] // 2
    blocks = lax.axis_size("sp")
    n_z = blocks // 4
    depth = out_weight.shape[1]
    halo = REACH * layers
    total = rows + halo
    bf, f32 = jnp.bfloat16, jnp.float32
    sends = 2 * (n_z - 1) + 3 + (n_z - 1) + n_z
    vmem = pl.BlockSpec(memory_space=pltpu.VMEM)
    return pl.pallas_call(
        functools.partial(kernel, n_z, layers, halo),
        out_shape=jax.ShapeDtypeStruct((rows, feats), bf),
        in_specs=[vmem] * 5,
        out_specs=vmem,
        scratch_shapes=[
            pltpu.VMEM((2 * layers, blocks, depth, feats), bf),
            pltpu.VMEM((total, feats), bf),
            pltpu.VMEM((total, feats), bf),
            pltpu.VMEM((halo, feats), bf),
            pltpu.VMEM((total, half), f32),
            pltpu.VMEM((layers, total, half), bf),
            pltpu.VMEM((layers, total, half), bf),
            pltpu.VMEM((layers, 2, total, half), bf),
            pltpu.VMEM((layers, total, 128), f32),
            pltpu.VMEM((layers, total, 128), f32),
            pltpu.SemaphoreType.DMA((2 * layers, sends)),
            pltpu.SemaphoreType.DMA((2 * layers, blocks)),
            pltpu.SemaphoreType.DMA((2 * layers,)),
            pltpu.SemaphoreType.DMA((1 + 3 * layers,)),
            pltpu.SemaphoreType.DMA((1 + 3 * layers,)),
        ],
        compiler_params=pltpu.CompilerParams(
            collective_id=0, has_side_effects=True, vmem_limit_bytes=60 * 1024 * 1024
        ),
    )(inputs, norm_gain, jnp.swapaxes(in_weight, 1, 2), pool_scale, out_weight)


def solution(mesh):
    n_sp, n_tp = mesh.shape["sp"], mesh.shape["tp"]
    fused = n_tp == 2 and n_sp == 16
    placed = (P("sp", "tp"), P(), P(None, "tp", "sp"), P(), P(None, "sp", "tp"))
    return jax.shard_map(
        fused_body if fused else plain_body,
        mesh=mesh, in_specs=placed, out_specs=P("sp", "tp"), check_vma=False,
    )
```

time: 328 us -> 180 us (0.55)
  the two profiles are of different devices: /device:TPU:4 before, /device:TPU:11 now
where the time goes in v1:
time: 180 us
  Pallas kernels  178 us (99%)
  local copies, waits for them, and re-layouts  2.3 us (1%)
    pallas_call x1, Pallas kernels, fused_body(): pl.pallas_call(functools.partial(kernel, n_z, layers, halo), out_shape=ja...  178 us

profile of v1, /device:TPU:11, one launch (start us, length us, event | category | flops | bytes accessed | tf_op | source)
XLA Modules:
  0.0 180.0 jit_solution(1902810909913171860)
XLA Ops:
  0.0 177.7 %shard_map.55 = bf16[256,2048]{1,0:T(8,128)(2,1)} custom-call(bf16[256,2048]{1,0:T(8,128)(2,1)} %x_ref.1, f32[3,4096]{1,0:T(4,128)} %gain_ref.1, bf16[3,64,2048]{2,1,0:T(8,128)(2,1)} %bitcast.1, f32[3,1024]{1,0:T(4,128)} %scale_ref.1, bf16[3,64,2048]{2,1,0:T(8,128)(2,1)} %wo_ref.1), custom_call_target="tpu_custom_call" | custom-call | tf_op jit(solution)/shard_map/pallas_call | solution.py:281
  177.7 2.3 %copy.7 = bf16[256,2048]{1,0:T(8,128)(2,1)} copy(bf16[256,2048]{1,0:T(8,128)(2,1)} %shard_map.55) | data formatting | bytes 2097152

commit v2 on v1

v2 whole, which is shorter than its diff:
```python
import functools

import jax
import jax.numpy as jnp
from jax import lax
from jax.experimental import pallas as pl
from jax.experimental.pallas import tpu as pltpu
from jax.sharding import PartitionSpec as P

EPS = 1e-06
REACH = 16
GROUPS = 4
MESH_ID = pl.DeviceIdType.MESH


def shift_sp(value):
    count = lax.axis_size("sp")
    return lax.ppermute(value, "sp", [(i, i + 1) for i in range(count - 1)])


def window_means(extended, row_count, first_channel, first_pos, pool_total):
    width = extended.shape[1]
    channel = first_channel + lax.broadcasted_iota(jnp.int32, (1, width), 1)
    window_len = jnp.left_shift(jnp.int32(2), channel // (pool_total // GROUPS))
    running = jnp.zeros((row_count, width), jnp.float32)
    for offset in range(REACH):
        shifted = extended[REACH - offset : REACH - offset + row_count]
        running = running + jnp.where(offset < window_len, shifted, 0.0)
    position = first_pos + lax.broadcasted_iota(jnp.int32, (row_count, 1), 0)
    divisor = jnp.minimum(position + 1, window_len).astype(jnp.float32)
    return running / divisor - extended[REACH:]


def plain_body(inputs, norm_gain, in_weight, pool_scale, out_weight):
    rows, feats = inputs.shape
    layers, features = norm_gain.shape
    pools = pool_scale.shape[1]
    part = pools // lax.axis_size("tp")
    t = lax.axis_index("tp")
    s = lax.axis_index("sp")
    current = inputs
    for layer in range(layers):
        in_all = lax.all_gather(in_weight[layer], "sp", axis=1, tiled=True)
        out_all = lax.all_gather(out_weight[layer], "sp", axis=0, tiled=True)
        wide = current.astype(jnp.float32)
        squares = lax.psum(jnp.sum(wide * wide, axis=1), "tp")
        inv_rms = lax.rsqrt(squares / features + EPS)[:, None]
        gain = lax.dynamic_slice_in_dim(norm_gain[layer], t * feats, feats)
        normed = (wide * inv_rms * gain).astype(jnp.bfloat16)
        partial = jnp.dot(normed, in_all, preferred_element_type=jnp.float32)
        pool_in = lax.psum_scatter(
            partial.astype(jnp.bfloat16), "tp", scatter_dimension=1, tiled=True
        )
        edge = shift_sp(pool_in[rows - REACH :])
        extended = jnp.concatenate([edge, pool_in], 0).astype(jnp.float32)
        means = window_means(extended, rows, t * part, s * rows, pools)
        scale = lax.dynamic_slice_in_dim(pool_scale[layer], t * part, part)
        mixed = (means * scale).astype(jnp.bfloat16)
        pooled = lax.all_gather(mixed, "tp", axis=1, tiled=True)
        branch = jnp.dot(pooled, out_all, preferred_element_type=jnp.float32)
        current = (current.astype(jnp.float32) + branch).astype(jnp.bfloat16)
    return current


def kernel(
    n_z, layers, halo,
    x_ref, gain_ref, wi_ref, scale_ref, wo_ref, o_ref,
    held, state, xg, edge, p_own, p_send, p_recv, mix, sq_send, sq_recv,
    w_send, w_recv, local_sem, a_send, a_recv,
):
    rows, feats = x_ref.shape
    total = rows + halo
    blocks = held.shape[1]
    half = mix.shape[2] * mix.shape[4]
    pools = 2 * half
    phases = 2 * layers
    s = lax.axis_index("sp")
    t = lax.axis_index("tp")
    core = s % 2
    y = (s // 2) % 2
    z = s // 4

    def block_of(zz, yy, cc):
        return zz * 4 + yy * 2 + cc

    upper = z // 2
    near = z + 1 - 2 * (z % 2)
    across = n_z // 2 - upper
    far = (n_z - 1) * (1 - upper)
    at_end = jnp.logical_or(z == 0, z == n_z - 1)
    inside = jnp.logical_not(at_end)
    up, down = (z + 1) % n_z, (z + n_z - 1) % n_z
    has_up, has_down = z < n_z - 1, z > 0
    inner = jnp.where(upper == 0, up, down)
    outer = jnp.where(upper == 0, down, up)

    y_mate = (block_of(z, 1 - y, core), t)
    c_mate = (block_of(z, y, 1 - core), t)
    x_mate = (s, 1 - t)
    after = ((s + 1) % blocks, t)
    before = ((s + blocks - 1) % blocks, t)

    def along(zz):
        return (block_of(zz, y, core), t)

    barrier = pltpu.get_barrier_semaphore()
    peers = [along(up), along(down), y_mate, c_mate, x_mate, after, before]
    for peer in peers:
        pl.semaphore_signal(barrier, inc=1, device_id=peer, device_id_type=MESH_ID)
    pl.semaphore_wait(barrier, len(peers))

    sent = []

    def send(src, dst, send_sem, recv_sem, to, when=None):
        copy = pltpu.make_async_remote_copy(
            src_ref=src, dst_ref=dst, send_sem=send_sem, recv_sem=recv_sem,
            device_id=to, device_id_type=MESH_ID,
        )
        if when is None:
            copy.start()
        else:
            pl.when(when)(copy.start)
        sent.append((copy, when))

    def arrived(ref, sem):
        pltpu.make_async_remote_copy(
            src_ref=ref, dst_ref=ref, send_sem=sem, recv_sem=sem,
            device_id=c_mate, device_id_type=MESH_ID,
        ).wait_recv()

    depth = held.shape[2]
    whole, first, second = pl.ds(0, depth), pl.ds(0, depth // 2), pl.ds(depth // 2, depth // 2)

    def own(p):
        return (wi_ref if p % 2 == 0 else wo_ref).at[p // 2]

    count = [0] * phases

    def send_own(p, to, when=None):
        send(own(p), held.at[p, s], w_send.at[p, count[p]], w_recv.at[p, s, 0], to, when)
        count[p] += 1

    def forward(p, block, to, piece=None, when=None):
        piece = whole if piece is None else piece
        ref = held.at[p, block, piece]
        sem = w_recv.at[p, block, 1 if piece is second else 0]
        send(ref, ref, w_send.at[p, count[p]], sem, to, when)
        count[p] += 1

    def wait_block(p, block, piece=None):
        piece = whole if piece is None else piece
        arrived(held.at[p, block, piece], w_recv.at[p, block, 1 if piece is second else 0])

    locals_ = []

    def issue_own(p):
        if p >= phases:
            return
        send_own(p, along(up), has_up)
        send_own(p, along(down), has_down)
        send_own(p, y_mate)
        send_own(p, c_mate)
        copy = pltpu.make_async_copy(own(p), held.at[p, s], local_sem.at[p])
        copy.start()
        locals_.append(copy)

    def take_mate(p):
        block = block_of(z, 1 - y, core)
        wait_block(p, block)
        forward(p, block, along(inner), second, at_end)
        forward(p, block, c_mate)

    def take_near(p):
        block = block_of(near, y, core)
        wait_block(p, block)
        forward(p, block, along(inner), None, inside)
        forward(p, block, y_mate, first)
        forward(p, block, y_mate, second, at_end)
        forward(p, block, c_mate)

    def take_across(p):
        block = block_of(across, y, core)
        wait_block(p, block)
        forward(p, block, along(outer), None, inside)
        forward(p, block, y_mate)
        forward(p, block, c_mate)

    def take_far(p):
        block = block_of(far, y, core)
        wait_block(p, block)
        forward(p, block, along(outer), None, inside)
        forward(p, block, y_mate, first)
        forward(p, block, c_mate)

    def take_mate_near(p):
        block = block_of(near, 1 - y, core)
        wait_block(p, block, second)
        forward(p, block, along(inner), second, inside)
        wait_block(p, block, first)
        forward(p, block, c_mate)

    def take_mate_across(p):
        block = block_of(across, 1 - y, core)
        wait_block(p, block)
        forward(p, block, c_mate)

    def take_mate_far(p):
        block = block_of(far, 1 - y, core)
        wait_block(p, block, second)
        forward(p, block, along(outer), second, inside)
        wait_block(p, block, first)
        forward(p, block, c_mate)

    def finish(p):
        locals_[p].wait()
        for zz in range(n_z):
            for yy in range(2):
                wait_block(p, block_of(zz, yy, 1 - core))

    send(x_ref.at[pl.ds(rows - halo, halo)], edge, a_send.at[0], a_recv.at[0], after)
    issue_own(0)
    issue_own(1)

    @pl.loop(0, rows // REACH)
    def _(i):
        state[pl.ds(halo + i * REACH, REACH)] = x_ref[pl.ds(i * REACH, REACH)]

    arrived(edge, a_recv.at[0])
    keep = (s > 0).astype(jnp.float32)

    @pl.loop(0, halo // REACH)
    def _(i):
        part = edge[pl.ds(i * REACH, REACH)].astype(jnp.float32) * keep
        state[pl.ds(i * REACH, REACH)] = part.astype(jnp.bfloat16)

    def first_row(layer):
        return REACH * layer

    def from_row(start):
        return pl.ds(start, total - start)

    parts = mix.shape[2]
    slim = mix.shape[4]
    ahead = blocks // (2 * parts)

    def exchange(src, dst, sem):
        send(src, dst, a_send.at[sem], a_recv.at[sem], x_mate)

    def base_sem(layer):
        return 1 + (1 + 2 * parts) * layer

    def squares(layer):
        @pl.loop(first_row(layer) // REACH, total // REACH)
        def _(i):
            at = pl.ds(i * REACH, REACH)
            wide = state[at].astype(jnp.float32)
            value = jnp.sum(wide * wide, axis=1, keepdims=True)
            sq_send[layer, at] = jnp.broadcast_to(value, (REACH, 128))
            gain = gain_ref[pl.ds(layer, 1), pl.ds(pl.multiple_of(t * feats, 128), feats)]
            xg[at] = (wide * gain).astype(jnp.bfloat16)

        at = from_row(first_row(layer))
        exchange(sq_send.at[layer, at], sq_recv.at[layer, at], base_sem(layer))

    def project(layer, which, c):
        block = which * (blocks // 2) + c * ahead
        weight = held[2 * layer, pl.ds(block, ahead)].reshape(slim, feats)
        return lax.dot_general(
            xg[first_row(layer):], weight, (((1,), (1,)), ((), ())),
            preferred_element_type=jnp.float32,
        )

    def project_other(layer, c):
        at = from_row(first_row(layer))
        p_send[layer, c, at] = project(layer, 1 - t, c).astype(jnp.bfloat16)
        exchange(p_send.at[layer, c, at], p_recv.at[layer, c, at], base_sem(layer) + 1 + c)

    def project_own(layer, c):
        p_own[c, from_row(first_row(layer))] = project(layer, t, c)

    def pool(layer, c):
        sem = base_sem(layer)
        start = first_row(layer)
        at = from_row(start)
        if c == 0:
            arrived(sq_recv.at[layer, at], a_recv.at[sem])
        arrived(p_recv.at[layer, c, at], a_recv.at[sem + 1 + c])
        lanes = 128
        row = lax.broadcasted_iota(jnp.int32, (total - start, lanes), 0)
        position = s * rows - halo + start + row
        mean = (sq_send[layer, at] + sq_recv[layer, at]) / (2 * feats)
        inv = lax.rsqrt(mean + EPS)
        for j in range(slim // lanes):
            cols = pl.ds(j * lanes, lanes)
            joined = p_own[c, at, cols].astype(jnp.bfloat16).astype(jnp.float32)
            joined = joined + p_recv[layer, c, at, cols].astype(jnp.float32)
            base = (joined * inv).astype(jnp.bfloat16).astype(jnp.float32)
            lane = t * half + c * slim + j * lanes
            channel = lane + lax.broadcasted_iota(jnp.int32, (1, lanes), 1)
            group = channel // (pools // GROUPS)
            running = base
            width = 1
            picked = None
            for g in range(GROUPS):
                running = running + pltpu.roll(running, width, 0)
                width *= 2
                picked = running if picked is None else jnp.where(group >= g, running, picked)
            span = jnp.left_shift(jnp.int32(2), group)
            divisor = jnp.maximum(jnp.minimum(position + 1, span), 1).astype(jnp.float32)
            scale = scale_ref[pl.ds(layer, 1), pl.ds(pl.multiple_of(lane, 128), lanes)]
            mix[layer, t, c, at, cols] = ((picked / divisor - base) * scale).astype(jnp.bfloat16)
        at = from_row(first_row(layer + 1))
        exchange(mix.at[layer, t, c, at], mix.at[layer, t, c, at], sem + 1 + parts + c)

    def take_mix(layer):
        at = from_row(first_row(layer + 1))
        for c in range(parts):
            arrived(mix.at[layer, 1 - t, c, at], a_recv.at[base_sem(layer) + 1 + parts + c])

    def expand(layer, start, stop):
        p = 2 * layer + 1
        width = 256
        last = layer == layers - 1
        at = from_row(first_row(layer + 1))

        @pl.loop(start, stop)
        def _(n):
            cols = pl.ds(pl.multiple_of(n * width, width), width)
            mixed = jnp.concatenate(
                [mix[layer, h, c, at] for h in range(2) for c in range(parts)], axis=1
            )
            weight = held[p, :, :, cols].reshape(pools, width)
            branch = jnp.dot(mixed, weight, preferred_element_type=jnp.float32)
            new = (state[at, cols].astype(jnp.float32) + branch).astype(jnp.bfloat16)
            if last:
                o_ref[:, cols] = new
            else:
                state[at, cols] = new

    part = functools.partial

    def pieces(p):
        layer = p // 2
        if p % 2 == 0:
            todo = [part(project_other, layer, c) for c in range(parts)]
            todo += [part(project_own, layer, c) for c in range(parts)]
            return todo + [part(pool, layer, c) for c in range(parts)]
        columns = feats // 256
        step = columns // 4
        todo = [part(take_mix, layer)]
        todo += [part(expand, layer, k, k + step) for k in range(0, columns, step)]
        if layer + 1 < layers:
            todo.append(part(squares, layer + 1))
        return todo

    order_first = [take_mate, take_near, take_across, take_far]
    order_then = [take_mate_near, take_mate_across, take_mate_far, finish]
    waiting = []

    def work():
        if waiting:
            piece = waiting.pop(0)
            if piece is not None:
                piece()

    squares(0)
    for take in order_first:
        take(0)
    for p in range(phases):
        issue_own(p + 2)
        for take in order_first[:2]:
            if p + 1 < phases:
                take(p + 1)
                work()
        for take in order_then[:2]:
            take(p)
            work()
        for take in order_first[2:]:
            if p + 1 < phases:
                take(p + 1)
                work()
        for take in order_then[2:]:
            take(p)
            work()
        waiting.extend(pieces(p))
        work()
        if p % 2 == 0:
            work()
            work()
            work()
    while waiting:
        work()
    for copy, when in sent:
        if when is None:
            copy.wait_send()
        else:
            pl.when(when)(copy.wait_send)


def fused_body(inputs, norm_gain, in_weight, pool_scale, out_weight):
    rows, feats = inputs.shape
    layers = norm_gain.shape[0]
    half = pool_scale.shape[1] // 2
    blocks = lax.axis_size("sp")
    n_z = blocks // 4
    depth = out_weight.shape[1]
    halo = REACH * layers
    total = rows + halo
    bf, f32 = jnp.bfloat16, jnp.float32
    sends = 21
    parts = 2
    slim = half // parts
    vmem = pl.BlockSpec(memory_space=pltpu.VMEM)
    return pl.pallas_call(
        functools.partial(kernel, n_z, layers, halo),
        out_shape=jax.ShapeDtypeStruct((rows, feats), bf),
        in_specs=[vmem] * 5,
        out_specs=vmem,
        scratch_shapes=[
            pltpu.VMEM((2 * layers, blocks, depth, feats), bf),
            pltpu.VMEM((total, feats), bf),
            pltpu.VMEM((total, feats), bf),
            pltpu.VMEM((halo, feats), bf),
            pltpu.VMEM((parts, total, slim), f32),
            pltpu.VMEM((layers, parts, total, slim), bf),
            pltpu.VMEM((layers, parts, total, slim), bf),
            pltpu.VMEM((layers, 2, parts, total, slim), bf),
            pltpu.VMEM((layers, total, 128), f32),
            pltpu.VMEM((layers, total, 128), f32),
            pltpu.SemaphoreType.DMA((2 * layers, sends)),
            pltpu.SemaphoreType.DMA((2 * layers, blocks, 2)),
            pltpu.SemaphoreType.DMA((2 * layers,)),
            pltpu.SemaphoreType.DMA((1 + (1 + 2 * parts) * layers,)),
            pltpu.SemaphoreType.DMA((1 + (1 + 2 * parts) * layers,)),
        ],
        compiler_params=pltpu.CompilerParams(
            collective_id=0, has_side_effects=True, vmem_limit_bytes=60 * 1024 * 1024
        ),
    )(inputs, norm_gain, jnp.swapaxes(in_weight, 1, 2), pool_scale, out_weight)


def solution(mesh):
    n_sp, n_tp = mesh.shape["sp"], mesh.shape["tp"]
    fused = n_tp == 2 and n_sp == 16
    placed = (P("sp", "tp"), P(), P(None, "tp", "sp"), P(), P(None, "sp", "tp"))
    return jax.shard_map(
        fused_body if fused else plain_body,
        mesh=mesh, in_specs=placed, out_specs=P("sp", "tp"), check_vma=False,
    )
```

time: 180 us -> 151 us (0.84)
  the two profiles are of different devices: /device:TPU:11 before, /device:TPU:4 now
where the time goes in v2:
time: 151 us; the launch traced here: 150 us
  Pallas kernels  148 us (98%)
  local copies, waits for them, and re-layouts  2.3 us (2%)
    pallas_call x1, Pallas kernels, fused_body(): pl.pallas_call(functools.partial(kernel, n_z, layers, halo), out_shape=ja...  148 us

profile of v2, /device:TPU:4, one launch (start us, length us, event | category | flops | bytes accessed | tf_op | source)
XLA Modules:
  0.0 149.9 jit_solution(4735187431852211860)
XLA Ops:
  0.0 147.5 %shard_map.55 = bf16[256,2048]{1,0:T(8,128)(2,1)} custom-call(bf16[256,2048]{1,0:T(8,128)(2,1)} %x_ref.1, f32[3,4096]{1,0:T(4,128)} %gain_ref.1, bf16[3,64,2048]{2,1,0:T(8,128)(2,1)} %bitcast.1, f32[3,1024]{1,0:T(4,128)} %scale_ref.1, bf16[3,64,2048]{2,1,0:T(8,128)(2,1)} %wo_ref.1), custom_call_target="tpu_custom_call" | custom-call | tf_op jit(solution)/shard_map/pallas_call | solution.py:414
  147.6 2.3 %copy.7 = bf16[256,2048]{1,0:T(8,128)(2,1)} copy(bf16[256,2048]{1,0:T(8,128)(2,1)} %shard_map.55) | data formatting | bytes 2097152
